TPU v7x, 32 devices: a whole 2x2x4 slice. The times are simulated.
32 devices in a mesh: ep: 8 (over z, core), tp: 4 (over y, x).
Axes of the slice: x: 2, y: 2, z: 4, core: 2. Of those that a mesh axis runs over, the one named last changes fastest.
Arguments:
- tokens: bfloat16 [256, 2048], P('ep'), may hold values from -6 to 6
- recurrent_head_state: float32 [256, 16, 4096], P('ep', 'tp'), may hold values from -4 to 4
- first_norm_gain: float32 [2048], replicated, may hold values from 0.1 to 1.9
- receptance_matrix: bfloat16 [2048, 1024], P(None, 'tp'), may hold values from -0.125 to 0.125
- key_matrix: bfloat16 [2048, 1024], P(None, 'tp'), may hold values from -0.125 to 0.125
- value_matrix: bfloat16 [2048, 1024], P(None, 'tp'), may hold values from -0.125 to 0.125
- decay_matrix: bfloat16 [2048, 1024], P(None, 'tp'), may hold values from -0.125 to 0.125
- decay_offset: float32 [1024], P('tp'), may hold values from -3 to 0.5
- correction_offset: float32 [1024], P('tp'), may hold values from -2 to 2
- correction_key_factor: float32 [1024], P('tp'), may hold values from -1 to 1
- own_term_weight: float32 [1024], P('tp'), may hold values from -0.9 to 0.9
- head_norm_gain: float32 [1024], P('tp'), may hold values from 0.1 to 1.9
- output_matrix: bfloat16 [1024, 2048], P('tp'), may hold values from -0.1875 to 0.1875
- second_norm_gain: float32 [2048], replicated, may hold values from 0.1 to 1.9
- routing: int32 [256, 2], replicated, may hold values from 0 to 7, all different within a row; in each aligned block of 32 rows (0 to 31, 32 to 63, ...) at most 16 rows name the same one
- routing_weight: float32 [256, 2], P('ep'), may hold values from 0.1 to 1
- expert_gate_weight: bfloat16 [8, 2048, 4096], P('ep', None, 'tp'), may hold values from -0.125 to 0.125
- expert_up_weight: bfloat16 [8, 2048, 4096], P('ep', None, 'tp'), may hold values from -0.125 to 0.125
- expert_down_weight: bfloat16 [8, 4096, 2048], P('ep', 'tp'), may hold values from -0.125 to 0.125
- dense_gate_weight: bfloat16 [2048, 2816], P(None, 'ep'), may hold values from -0.125 to 0.125
- dense_up_weight: bfloat16 [2048, 2816], P(None, 'ep'), may hold values from -0.125 to 0.125
- dense_down_weight: bfloat16 [2816, 2048], P('ep'), may hold values from -0.109375 to 0.109375
- dense_gate_offset: float32 [2048], replicated, may hold values from -3 to 3
Outputs:
- layer_out: bfloat16 [256, 2048], P(('ep', 'tp'))
- next_state: float32 [256, 16, 4096], P('ep', 'tp')
Inputs may be any that keep to these rules, and one draw needn't show every extreme that they name: `routing`: each row names 2 different experts. In each aligned block of 32 rows no expert is named more than 16 times, a bound that some block reaches.
All inputs are finite; a program needn't handle non-finite values.
Results may differ from a plain program's by a relative error of at most 0.017.
Values may be sent and summed in bfloat16 or wider, within the bound.
A program may use at most 64 MiB of HBM per device.

v0:
```python
import jax
import jax.numpy as jnp
from jax import lax
from jax.sharding import PartitionSpec as P

HEAD_WIDTH = 64
PRECISE = lax.Precision.HIGHEST


def rms_scale(rows, gain):
    floats = rows.astype(jnp.float32)
    return floats * lax.rsqrt(jnp.mean(floats * floats, axis=-1, keepdims=True) + 1e-06) * gain


def route_table(block_routes, experts, capacity):
    flat_routes = block_routes.reshape(-1)
    chosen = (flat_routes[:, None] == jnp.arange(experts, dtype=jnp.int32)[None, :]).astype(
        jnp.int32
    )
    before = jnp.cumsum(chosen, axis=0, dtype=jnp.int32) - chosen
    slot_index = jnp.sum(before * chosen, axis=1)
    slot_match = (slot_index[:, None] == jnp.arange(capacity, dtype=jnp.int32)[None, :]).astype(
        jnp.float32
    )
    dispatch_table = chosen.astype(jnp.float32)[:, :, None] * slot_match[:, None, :]
    return dispatch_table.reshape(block_routes.shape[0], block_routes.shape[1], experts, capacity)


def state_update(
    receptance_rows,
    key_matrix_rows,
    value_matrix_rows,
    decay_logits,
    recurrent_head_state,
    decay_offset,
    correction_offset,
    correction_key_factor,
    own_term_weight,
    head_norm_gain,
    head_width,
):
    seq_count = key_matrix_rows.shape[0]
    decay_factor = jnp.exp(-jnp.exp(decay_offset + decay_logits))
    in_rate = jax.nn.sigmoid(correction_offset + correction_key_factor * key_matrix_rows)
    key_in = key_matrix_rows * in_rate

    def split_heads(block):
        return block.reshape(seq_count, -1, head_width)

    keys_head = split_heads(key_matrix_rows)
    unit_keys = (
        keys_head
        * lax.rsqrt(jnp.mean(keys_head * keys_head, axis=-1, keepdims=True) + 1e-06)
        * head_width ** (-0.5)
    )
    rate_head = split_heads(in_rate)
    head_keys = split_heads(key_in)
    decay_head = split_heads(decay_factor)
    head_values = split_heads(value_matrix_rows)
    head_receptance = split_heads(receptance_rows)
    matrix = recurrent_head_state.reshape(seq_count, -1, head_width, head_width)
    removed = jnp.einsum("bhvk,bhk->bhv", matrix, unit_keys, precision=PRECISE)
    updated = (
        matrix * decay_head[:, :, None, :]
        - removed[..., None] * (unit_keys * rate_head)[:, :, None, :]
        + head_values[..., None] * head_keys[:, :, None, :]
    )
    readout = jnp.einsum("bhvk,bhk->bhv", updated, head_receptance, precision=PRECISE)
    center = jnp.mean(readout, axis=-1, keepdims=True)
    spread = jnp.mean(jnp.square(readout - center), axis=-1, keepdims=True)
    normalized_rows = (
        (readout - center) * lax.rsqrt(spread + 0.00064) * head_norm_gain.reshape(-1, head_width)
    )
    own_term_total = jnp.sum(
        head_receptance * head_keys * own_term_weight.reshape(-1, head_width),
        axis=-1,
        keepdims=True,
    )
    normalized_rows = normalized_rows + own_term_total * head_values
    return (
        normalized_rows.reshape(seq_count, -1).astype(jnp.bfloat16),
        updated.reshape(seq_count, -1, head_width * head_width),
    )


def local(
    tokens,
    recurrent_head_state,
    first_norm_gain,
    receptance_matrix,
    key_matrix,
    value_matrix,
    decay_matrix,
    decay_offset,
    correction_offset,
    correction_key_factor,
    own_term_weight,
    head_norm_gain,
    output_matrix,
    second_norm_gain,
    routing,
    routing_weight,
    expert_gate_weight,
    expert_up_weight,
    expert_down_weight,
    dense_gate_weight,
    dense_up_weight,
    dense_down_weight,
    dense_gate_offset,
):
    seq_count = tokens.shape[0]
    width = tokens.shape[1]
    group_index = lax.axis_index("ep")
    lane_index = lax.axis_index("tp")
    group_count = lax.axis_size("ep")
    lane_count = lax.axis_size("tp")
    normalized_rows = rms_scale(tokens, first_norm_gain).astype(jnp.bfloat16)
    receptance_rows = jnp.dot(
        normalized_rows, receptance_matrix, preferred_element_type=jnp.float32
    )
    key_matrix_rows = jnp.dot(normalized_rows, key_matrix, preferred_element_type=jnp.float32)
    value_matrix_rows = jnp.dot(normalized_rows, value_matrix, preferred_element_type=jnp.float32)
    decay_logits = jnp.dot(normalized_rows, decay_matrix, preferred_element_type=jnp.float32)
    head_outputs, next_state = state_update(
        receptance_rows,
        key_matrix_rows,
        value_matrix_rows,
        decay_logits,
        recurrent_head_state,
        decay_offset,
        correction_offset,
        correction_key_factor,
        own_term_weight,
        head_norm_gain,
        HEAD_WIDTH,
    )
    partial_out = jnp.dot(head_outputs, output_matrix, preferred_element_type=jnp.float32)
    hidden_sum = tokens.astype(jnp.float32) + lax.psum(
        partial_out.astype(jnp.bfloat16), "tp"
    ).astype(jnp.float32)
    ffn_in = rms_scale(hidden_sum, second_norm_gain).astype(jnp.bfloat16)
    local_experts = expert_gate_weight.shape[0]
    top_count = routing.shape[1]
    expert_count = local_experts * group_count
    capacity = 2 * seq_count * top_count // expert_count
    per_lane = seq_count // lane_count
    own_routes = lax.dynamic_slice_in_dim(routing, group_index * seq_count, seq_count, 0)
    own_table = route_table(own_routes, expert_count, capacity)
    send_rows = jnp.einsum(
        "bkec,bd->ecd", own_table.astype(jnp.bfloat16), ffn_in, preferred_element_type=jnp.float32
    ).astype(jnp.bfloat16)
    lane_rows = lax.dynamic_slice_in_dim(ffn_in, lane_index * per_lane, per_lane, 0)
    dense_send = jnp.broadcast_to(lane_rows[None], (group_count, per_lane, width))
    expert_in, dense_in = (
        lax.all_to_all(send_rows, "ep", split_axis=0, concat_axis=0, tiled=True),
        lax.all_to_all(dense_send, "ep", split_axis=0, concat_axis=0, tiled=True),
    )
    rows_in = expert_in.reshape(group_count, local_experts, capacity, width).transpose(1, 0, 2, 3)
    rows_in = rows_in.reshape(local_experts, group_count * capacity, width)
    gate_pre = jnp.einsum(
        "lrd,ldf->lrf", rows_in, expert_gate_weight, preferred_element_type=jnp.float32
    )
    up_pre = jnp.einsum(
        "lrd,ldf->lrf", rows_in, expert_up_weight, preferred_element_type=jnp.float32
    )
    expert_hidden = (jax.nn.silu(gate_pre) * up_pre).astype(jnp.bfloat16)
    expert_part = jnp.einsum(
        "lrf,lfd->lrd", expert_hidden, expert_down_weight, preferred_element_type=jnp.float32
    )
    expert_out = lax.psum_scatter(
        expert_part.astype(jnp.bfloat16), "tp", scatter_dimension=2, tiled=True
    )
    back_send = expert_out.reshape(local_experts, group_count, capacity, -1).transpose(1, 0, 2, 3)
    back_send = back_send.reshape(group_count * local_experts, capacity, -1)
    dense_rows = dense_in.reshape(group_count * per_lane, width)
    dense_hidden = (
        jax.nn.silu(jnp.dot(dense_rows, dense_gate_weight, preferred_element_type=jnp.float32))
        * jnp.dot(dense_rows, dense_up_weight, preferred_element_type=jnp.float32)
    ).astype(jnp.bfloat16)
    dense_part = jnp.dot(
        dense_hidden, dense_down_weight, preferred_element_type=jnp.float32
    ).astype(jnp.bfloat16)
    dense_part = dense_part.reshape(group_count, per_lane, width)
    back_experts, back_dense = (
        lax.all_to_all(back_send, "ep", split_axis=0, concat_axis=0, tiled=True),
        lax.all_to_all(dense_part, "ep", split_axis=0, concat_axis=0, tiled=True),
    )
    dense_sum = jnp.sum(back_dense.astype(jnp.float32), axis=0)
    weighted = jnp.einsum("bkec,bk->ecb", own_table, routing_weight, precision=PRECISE)
    moe_slice = jnp.einsum(
        "ecb,ecd->bd", weighted, back_experts.astype(jnp.float32), precision=PRECISE
    )
    moe_rows = lax.all_to_all(moe_slice, "tp", split_axis=0, concat_axis=1, tiled=True)
    residual_rows = lax.dynamic_slice_in_dim(hidden_sum, lane_index * per_lane, per_lane, 0)
    layer_out = (residual_rows + moe_rows + jax.nn.sigmoid(dense_gate_offset) * dense_sum).astype(
        jnp.bfloat16
    )
    return (layer_out, next_state)


def solution(mesh):
    return jax.shard_map(
        local,
        mesh=mesh,
        in_specs=(
            P("ep", None),
            P("ep", "tp", None),
            P(),
            P(None, "tp"),
            P(None, "tp"),
            P(None, "tp"),
            P(None, "tp"),
            P("tp"),
            P("tp"),
            P("tp"),
            P("tp"),
            P("tp"),
            P("tp", None),
            P(),
            P(),
            P("ep", None),
            P("ep", None, "tp"),
            P("ep", None, "tp"),
            P("ep", "tp", None),
            P(None, "ep"),
            P(None, "ep"),
            P("ep", None),
            P(),
        ),
        out_specs=(P(("ep", "tp"), None), P("ep", "tp", None)),
        check_vma=False,
    )
```

profile of v0, /device:TPU:0, one launch (start us, length us, event | category | flops | bytes accessed | tf_op | source)
XLA Modules:
  0.0 217.0 jit_solution(15776234293525649654)
XLA Ops:
  31.4 3.3 %reshape.173 = f32[32,4,64,64]{3,2,1,0:T(8,128)} reshape(f32[32,4,4096]{2,1,0:T(4,128)S(1)} %copy-done.2) | data formatting | bytes 4194304 | tf_op jit(solution)/shard_map/reshape | solution.py:61
  35.9 8.6 %fusion.70 = f32[32,4,1,64]{3,2,1,0:T(1,128)S(1)} fusion(f32[32,4,64,1]{2,3,1,0:T(1,128)S(1)} %bitcast.86, f32[32,4,64,64]{3,2,1,0:T(8,128)} %reshape.173), kind=kOutput, calls=%fused_computation.92 | convolution fusion | flops 6291456 | bytes 2162688 | tf_op jit(solution)/shard_map/bhvk,bhk->bhv/dot_general | solution.py:62
  44.5 9.0 %fusion.7 = f32[32,4,1,64]{3,2,1,0:T(1,128)} fusion(f32[32,4,64,1]{2,3,1,0:T(1,128)S(1)} %bitcast.92, f32[32,4,64,64]{3,2,1,0:T(8,128)S(1)} %copy-done.1, f32[32,4,64]{2,1,0:T(4,128)S(1)} %copy-done.6, f32[32,4,64]{2,1,0:T(4,128)S(1)} %get-tuple-element.4, f32[32,4,64]{2,1,0:T(4,128)S(1)} %bitcast.84, f32[32,4,64]{2,1,0:T(4,128)S(1)} %copy-done.8, ...), kind=kOutput, calls=%fused_computation.7 | convolution fusion | flops 8912896 | bytes 2326528 | tf_op jit(solution)/shard_map/bhvk,bhk->bhv/dot_general | solution.py:68
  71.6 34.1 %all-reduce.2.cloned.1.call-done = bf16[32,2048]{1,0:T(8,128)(2,1)} async-done(((bf16[32,2048]{1,0:T(8,128)(2,1)}), bf16[32,2048]{1,0:T(8,128)(2,1)}) %all-reduce.2.cloned.1.call-update) | async-done | bytes 131088 | tf_op jit(solution)/shard_map/psum | solution.py:138
  111.1 4.6 %all-to-all-start = ((bf16[8,16,2048]{2,1,0:T(8,128)(2,1)}), bf16[8,16,2048]{2,1,0:T(8,128)(2,1)}, u32[]{:S(2)}, u32[]{:S(2)}) async-start(bf16[8,16,2048]{2,1,0:T(8,128)(2,1)} %convolution_convert_fusion), calls=%async_computation | async-start | bytes 1048576 | tf_op jit(solution)/shard_map/all_to_all | solution.py:155
  115.8 15.4 %all-to-all-done = bf16[8,16,2048]{2,1,0:T(8,128)(2,1)} async-done(((bf16[8,16,2048]{2,1,0:T(8,128)(2,1)}), bf16[8,16,2048]{2,1,0:T(8,128)(2,1)}, u32[]{:S(2)}, u32[]{:S(2)}) %all-to-all-start) | async-done | bytes 524320 | tf_op jit(solution)/shard_map/all_to_all | solution.py:155
  131.2 3.9 %fusion.5 = f32[128,1024]{1,0:T(8,128)} fusion(bf16[128,2048]{1,0:T(8,128)(2,1)} %bitcast.9, bf16[1,2048,1024]{2,1,0:T(8,128)(2,1)} %param.39), kind=kOutput, calls=%fused_computation.5 | convolution fusion | flops 536870912 | bytes 5242880 | tf_op jit(solution)/shard_map/lrd,ldf->lrf/dot_general | solution.py:160
  135.0 6.0 %fusion.14 = bf16[1,128,2048]{2,1,0:T(8,128)(2,1)} fusion(bf16[1,1024,2048]{2,1,0:T(8,128)(2,1)} %param.41, bf16[128,2048]{1,0:T(8,128)(2,1)} %bitcast.9, bf16[1,2048,1024]{2,1,0:T(8,128)(2,1)} %param.40, f32[128,1024]{1,0:T(8,128)} %fusion.5), kind=kOutput, calls=%fused_computation.13 | convolution fusion | flops 1074790400 | bytes 9961472 | tf_op jit(solution)/shard_map/lrf,lfd->lrd/dot_general | solution.py:167
  142.5 4.2 %all-to-all-start.3 = ((bf16[8,8,2048]{2,1,0:T(8,128)(2,1)}), bf16[8,8,2048]{2,1,0:T(8,128)(2,1)}, u32[]{:S(2)}, u32[]{:S(2)}) async-start(bf16[8,8,2048]{2,1,0:T(8,128)(2,1)} %broadcast_in_dim.2), calls=%async_computation.4 | async-start | bytes 524288 | tf_op jit(solution)/shard_map/all_to_all | solution.py:156
  146.8 3.8 %broadcast_multiply_fusion = f32[32,4,64,64]{3,2,1,0:T(8,128)} fusion(f32[32,4,64]{2,1,0:T(4,128)} %mul.243, f32[32,4,64]{2,1,0:T(4,128)} %mul.240), kind=kLoop, calls=%fused_computation.18 | loop fusion | flops 524288 | bytes 2162688 | tf_op jit(solution)/shard_map/mul | solution.py:66
  150.6 5.1 %mul.277 = f32[32,4,4096]{2,1,0:T(4,128)} reshape(f32[32,4,64,64]{3,2,1,0:T(8,128)} %broadcast_multiply_fusion) | data formatting | bytes 4194304 | tf_op jit(solution)/shard_map/mul | solution.py:66
  155.6 3.8 %broadcast_multiply_fusion.1 = f32[32,4,64,64]{3,2,1,0:T(8,128)} fusion(f32[32,4,64]{2,1,0:T(4,128)} %copy-done.5, f32[32,4,64]{2,1,0:T(4,128)} %bitcast.85), kind=kLoop, calls=%fused_computation.19 | loop fusion | flops 524288 | bytes 2162688 | tf_op jit(solution)/shard_map/mul | solution.py:65
  159.4 5.0 %mul.276 = f32[32,4,4096]{2,1,0:T(4,128)} reshape(f32[32,4,64,64]{3,2,1,0:T(8,128)} %broadcast_multiply_fusion.1) | data formatting | bytes 4194304 | tf_op jit(solution)/shard_map/mul | solution.py:65
  164.5 3.0 %mul.227 = f32[32,4,64,64]{3,2,1,0:T(8,128)} broadcast(f32[32,4,64]{2,1,0:T(4,128)} %mul.226), dimensions={0,1,3} | broadcast | bytes 2129920 | tf_op jit(solution)/shard_map/mul | solution.py:64
  167.5 5.0 %mul.274 = f32[32,4,4096]{2,1,0:T(4,128)} reshape(f32[32,4,64,64]{3,2,1,0:T(8,128)} %mul.227) | data formatting | bytes 4194304 | tf_op jit(solution)/shard_map/mul | solution.py:64
  172.5 2.6 %fusion.44 = f32[64,352]{1,0:T(8,128)} fusion(bf16[2048,352]{0,1:T(8,128)(2,1)} %param.42, bf16[8,8,2048]{2,1,0:T(8,128)(2,1)} %all-to-all-done.3), kind=kOutput, calls=%fused_computation.46 | convolution fusion | flops 92274688 | bytes 1794048 | tf_op jit(solution)/shard_map/dot_general | solution.py:177
  175.2 4.8 %all-to-all-start.1 = ((bf16[8,16,512]{2,1,0:T(8,128)(2,1)}), bf16[8,16,512]{2,1,0:T(8,128)(2,1)}, u32[]{:S(2)}, u32[]{:S(2)}) async-start(bf16[8,16,512]{2,1,0:T(8,128)(2,1)} %bitcast.91), calls=%async_computation.2 | async-start | bytes 262144 | tf_op jit(solution)/shard_map/all_to_all | solution.py:185
  180.0 3.3 %fusion.17 = bf16[8,8,2048]{2,1,0:T(8,128)(2,1)} fusion(bf16[352,2048]{1,0:T(8,128)(2,1)S(1)} %copy-done, bf16[2048,352]{0,1:T(8,128)(2,1)} %param.43, bf16[8,8,2048]{2,1,0:T(8,128)(2,1)} %all-to-all-done.3, f32[64,352]{1,0:T(8,128)} %fusion.44), kind=kOutput, calls=%fused_computation.15 | convolution fusion | flops 184815616 | bytes 3497984 | tf_op jit(solution)/shard_map/dot_general | solution.py:180
  183.3 3.5 %all-to-all-done.1 = bf16[8,16,512]{2,1,0:T(8,128)(2,1)} async-done(((bf16[8,16,512]{2,1,0:T(8,128)(2,1)}), bf16[8,16,512]{2,1,0:T(8,128)(2,1)}, u32[]{:S(2)}, u32[]{:S(2)}) %all-to-all-start.1) | async-done | bytes 131104 | tf_op jit(solution)/shard_map/all_to_all | solution.py:185
  186.8 4.0 %all-to-all-start.4 = ((bf16[8,8,2048]{2,1,0:T(8,128)(2,1)}), bf16[8,8,2048]{2,1,0:T(8,128)(2,1)}, u32[]{:S(2)}, u32[]{:S(2)}) async-start(bf16[8,8,2048]{2,1,0:T(8,128)(2,1)} %fusion.17), calls=%async_computation.5 | async-start | bytes 524288 | tf_op jit(solution)/shard_map/all_to_all | solution.py:186
  190.9 4.7 %subtract_add_fusion = f32[16,8,4096]{2,1,0:T(8,128)} fusion(f32[16,8,4096]{2,1,0:T(8,128)} %bitcast.80, f32[16,8,4096]{2,1,0:T(8,128)} %bitcast.81, f32[16,8,4096]{2,1,0:T(8,128)S(1)} %bitcast.79, f32[16,8,4096]{2,1,0:T(8,128)} %bitcast.82), kind=kLoop, calls=%fused_computation.17 | loop fusion | flops 1572864 | bytes 10485760 | tf_op jit(solution)/shard_map/add | solution.py:64
  197.4 3.2 %all-to-all-done.4 = bf16[8,8,2048]{2,1,0:T(8,128)(2,1)} async-done(((bf16[8,8,2048]{2,1,0:T(8,128)(2,1)}), bf16[8,8,2048]{2,1,0:T(8,128)(2,1)}, u32[]{:S(2)}, u32[]{:S(2)}) %all-to-all-start.4) | async-done | bytes 262176 | tf_op jit(solution)/shard_map/all_to_all | solution.py:186
  200.6 3.3 %all-to-all-start.2 = ((f32[4,8,512]{2,1,0:T(8,128)}), f32[4,8,512]{2,1,0:T(8,128)S(1)}, u32[]{:S(2)}, u32[]{:S(2)}) async-start(f32[4,8,512]{2,1,0:T(8,128)} %convolution_bitcast_fusion), calls=%async_computation.3 | async-start | bytes 131072 | tf_op jit(solution)/shard_map/all_to_all | solution.py:193
  204.9 3.8 %all-to-all-done.2 = f32[4,8,512]{2,1,0:T(8,128)S(1)} async-done(((f32[4,8,512]{2,1,0:T(8,128)}), f32[4,8,512]{2,1,0:T(8,128)S(1)}, u32[]{:S(2)}, u32[]{:S(2)}) %all-to-all-start.2) | async-done | bytes 65568 | tf_op jit(solution)/shard_map/all_to_all | solution.py:193
  (80 shorter events, 54.6 us)
Async XLA Ops:
  7.2 172.8 %copy-start = (bf16[352,2048]{1,0:T(8,128)(2,1)S(1)}, bf16[352,2048]{1,0:T(8,128)(2,1)}, u32[]{:S(2)}) copy-start(bf16[352,2048]{1,0:T(8,128)(2,1)} %param.44) | copy-start | bytes 4325380
  7.2 16.7 %copy-start.10 = (f32[2048]{0:T(1024)S(1)}, f32[2048]{0:T(1024)}, u32[]{:S(2)}) copy-start(f32[2048]{0:T(1024)} %param.25) | copy-start | bytes 24580
  7.2 16.7 %copy-start.13 = (f32[256]{0:T(256)S(1)}, f32[256]{0:T(256)}, u32[]{:S(2)}) copy-start(f32[256]{0:T(256)} %param.32) | copy-start | bytes 3076
  7.2 24.2 %copy-start.2 = (f32[32,4,4096]{2,1,0:T(4,128)S(1)}, f32[32,4,4096]{2,1,0:T(4,128)}, u32[]{:S(2)}) copy-start(f32[32,4,4096]{2,1,0:T(4,128)} %param.24) | copy-start | bytes 6291460
  7.2 98.5 %all-reduce.2.cloned.1.call-start = ((), (), s32[]{:S(2)}) async-start(), calls=%async_computation.6 | async-start | bytes 262144 | tf_op jit(solution)/shard_map/psum | solution.py:138
  34.7 9.7 %copy-start.1 = (f32[32,4,64,64]{3,2,1,0:T(8,128)S(1)}, f32[32,4,64,64]{3,2,1,0:T(8,128)}, u32[]{:S(2)}) copy-start(f32[32,4,64,64]{3,2,1,0:T(8,128)} %reshape.173) | copy-start | bytes 6291460
  34.7 9.8 %copy-start.6 = (f32[32,4,64]{2,1,0:T(4,128)S(1)}, f32[32,4,64]{2,1,0:T(4,128)}, u32[]{:S(2)}) copy-start(f32[32,4,64]{2,1,0:T(4,128)} %mul.226) | copy-start | bytes 98308
  34.7 9.8 %copy-start.7 = (f32[32,4,64]{2,1,0:T(4,128)S(1)}, f32[32,4,64]{2,1,0:T(4,128)}, u32[]{:S(2)}) copy-start(f32[32,4,64]{2,1,0:T(4,128)} %mul.240) | copy-start | bytes 98308
  34.7 9.8 %copy-start.8 = (f32[32,4,64]{2,1,0:T(4,128)S(1)}, f32[32,4,64]{2,1,0:T(4,128)}, u32[]{:S(2)}) copy-start(f32[32,4,64]{2,1,0:T(4,128)} %mul.243) | copy-start | bytes 98308
  34.7 9.8 %copy-start.11 = (f32[32,4,64,1]{2,1,0,3:T(4,128)S(1)}, f32[32,4,64,1]{2,1,0,3:T(4,128)}, u32[]{:S(2)}) copy-start(f32[32,4,64,1]{2,1,0,3:T(4,128)} %reshape.185) | copy-start | bytes 98308
  35.9 17.6 %copy-start.5 = (f32[32,4,64]{2,1,0:T(4,128)}, f32[32,4,64]{2,1,0:T(4,128)S(1)}, u32[]{:S(2)}) copy-start(f32[32,4,64]{2,1,0:T(4,128)S(1)} %get-tuple-element.4) | copy-start | bytes 98308
  44.5 9.0 %copy-start.4 = (f32[32,4,1,64]{3,2,1,0:T(1,128)}, f32[32,4,1,64]{3,2,1,0:T(1,128)S(1)}, u32[]{:S(2)}) copy-start(f32[32,4,1,64]{3,2,1,0:T(1,128)S(1)} %fusion.70) | copy-start | bytes 98308
  108.6 0.7 copy-start.3
  111.1 20.0 %all-to-all-start = ((bf16[8,16,2048]{2,1,0:T(8,128)(2,1)}), bf16[8,16,2048]{2,1,0:T(8,128)(2,1)}, u32[]{:S(2)}, u32[]{:S(2)}) async-start(bf16[8,16,2048]{2,1,0:T(8,128)(2,1)} %convolution_convert_fusion), calls=%async_computation | async-start | bytes 1048576 | tf_op jit(solution)/shard_map/all_to_all | solution.py:155
  115.7 59.4 %reduce-scatter.2.cloned.1.call-start = ((), (), s32[]{:S(2)}) async-start(), calls=%async_computation.7 | async-start | bytes 655360 | tf_op jit(solution)/shard_map/reduce_scatter | solution.py:170
  142.5 30.0 %all-to-all-start.3 = ((bf16[8,8,2048]{2,1,0:T(8,128)(2,1)}), bf16[8,8,2048]{2,1,0:T(8,128)(2,1)}, u32[]{:S(2)}, u32[]{:S(2)}) async-start(bf16[8,8,2048]{2,1,0:T(8,128)(2,1)} %broadcast_in_dim.2), calls=%async_computation.4 | async-start | bytes 524288 | tf_op jit(solution)/shard_map/all_to_all | solution.py:156
  175.2 11.7 %all-to-all-start.1 = ((bf16[8,16,512]{2,1,0:T(8,128)(2,1)}), bf16[8,16,512]{2,1,0:T(8,128)(2,1)}, u32[]{:S(2)}, u32[]{:S(2)}) async-start(bf16[8,16,512]{2,1,0:T(8,128)(2,1)} %bitcast.91), calls=%async_computation.2 | async-start | bytes 262144 | tf_op jit(solution)/shard_map/all_to_all | solution.py:185
  186.8 13.8 %all-to-all-start.4 = ((bf16[8,8,2048]{2,1,0:T(8,128)(2,1)}), bf16[8,8,2048]{2,1,0:T(8,128)(2,1)}, u32[]{:S(2)}, u32[]{:S(2)}) async-start(bf16[8,8,2048]{2,1,0:T(8,128)(2,1)} %fusion.17), calls=%async_computation.5 | async-start | bytes 524288 | tf_op jit(solution)/shard_map/all_to_all | solution.py:186
  190.9 4.8 %copy-start.12 = (f32[2048]{0:T(1024)S(1)}, f32[2048]{0:T(1024)}, u32[]{:S(2)}) copy-start(f32[2048]{0:T(1024)} %param.45) | copy-start | bytes 24580
  190.9 4.8 %copy-start.9 = (f32[32,8,16]{0,2,1:T(8,128)S(1)}, f32[32,8,16]{0,2,1:T(8,128)}, u32[]{:S(2)}) copy-start(f32[32,8,16]{0,2,1:T(8,128)} %get-tuple-element.2) | copy-start | bytes 49156
  200.6 8.1 %all-to-all-start.2 = ((f32[4,8,512]{2,1,0:T(8,128)}), f32[4,8,512]{2,1,0:T(8,128)S(1)}, u32[]{:S(2)}, u32[]{:S(2)}) async-start(f32[4,8,512]{2,1,0:T(8,128)} %convolution_bitcast_fusion), calls=%async_computation.3 | async-start | bytes 131072 | tf_op jit(solution)/shard_map/all_to_all | solution.py:193
Sparse Core Ops, SparseCore 0:
  60.7 44.9 all-reduce.1
  141.2 23.0 reduce-scatter.1
where the time goes:
time: 219 us; the launch traced here: 217 us
  waiting for transfers between devices  60.1 us (27%)
  matrix products  48.1 us (22%)
  local copies, waits for them, and re-layouts  41.5 us (19%)
  other arithmetic  32 us (15%)
  starting transfers between devices  21 us (10%)
  between operations  14.3 us (7%)
    psum x1, waiting for transfers between devices, local(): lax.psum(partial_out.astype(jnp.bfloat16), 'tp').astype(jnp.float32)  34.1 us
    all_to_all x1, waiting for transfers between devices, local(): lax.all_to_all(send_rows, 'ep', split_axis=0, concat_axis=0, tiled=True)  15.4 us
    mul x3, local copies, waits for them, and re-layouts, state_update(): matrix * decay_head[:, :, None, :]  9.51 us
    dot_general x1, matrix products, state_update(): jnp.einsum('bhvk,bhk->bhv', updated, head_receptance, precision=PRECISE)  8.96 us
    dot_general x1, matrix products, state_update(): removed = jnp.einsum('bhvk,bhk->bhv', matrix, unit_keys, precision=PRECISE)  8.58 us
    mul x3, local copies, waits for them, and re-layouts, state_update(): head_values[..., None] * head_keys[:, :, None, :]  7.99 us
    dot_general x1, matrix products, local(): jnp.einsum('lrf,lfd->lrd', expert_hidden, expert_down_weight, preferred_e...  5.98 us
    reshape x4, local copies, waits for them, and re-layouts, split_heads(): return block.reshape(seq_count, -1, head_width)  5.88 us
  transfers between devices with their start and end apart: 7, of which 5 were waited for; matrix products, arithmetic and copies ran while one was open for 24% of the time, Pallas kernels for 0%

commit v1 on v0

--- a/solution.py
+++ b/solution.py
@@ -135,8 +135,8 @@
         HEAD_WIDTH,
     )
     partial_out = jnp.dot(head_outputs, output_matrix, preferred_element_type=jnp.float32)
-    hidden_sum = tokens.astype(jnp.float32) + lax.psum(
-        partial_out.astype(jnp.bfloat16), "tp"
+    hidden_sum = tokens.astype(jnp.float32) + jnp.sum(
+        lax.all_gather(partial_out.astype(jnp.bfloat16), "tp"), axis=0
     ).astype(jnp.float32)
     ffn_in = rms_scale(hidden_sum, second_norm_gain).astype(jnp.bfloat16)
     local_experts = expert_gate_weight.shape[0]

time: 219 us -> 197 us (0.90)
  waiting for transfers between devices: 60.1 us -> 25.9 us
  blocking collectives: 0 us -> 12.2 us
    psum x1 -> x0, waiting for transfers between devices: 34.1 us -> none  [local(): lax.psum(partial_out.astype(jnp.bfloat16), 'tp').astype(jnp.float32)]
    all_gather x0 -> x1, blocking collectives: none -> 12.2 us  [local(): lax.all_gather(partial_out.astype(jnp.bfloat16), 'tp')]
  transfers between devices with their start and end apart: 7 -> 6, of which waited for: 5 -> 4; matrix products, arithmetic and copies ran while one was open for 24% -> 21% of each run, Pallas kernels for 0% -> 0%
where the time goes in v1:
time: 197 us; the launch traced here: 195 us
  matrix products  46.7 us (24%)
  local copies, waits for them, and re-layouts  41.3 us (21%)
  other arithmetic  33 us (17%)
  waiting for transfers between devices  25.9 us (13%)
  starting transfers between devices  21.3 us (11%)
  between operations  14.3 us (7%)
  blocking collectives  12.2 us (6%)
    all_to_all x1, waiting for transfers between devices, local(): lax.all_to_all(send_rows, 'ep', split_axis=0, concat_axis=0, tiled=True)  15.4 us
    all_gather x1, blocking collectives, local(): lax.all_gather(partial_out.astype(jnp.bfloat16), 'tp')  12.2 us
    mul x3, local copies, waits for them, and re-layouts, state_update(): matrix * decay_head[:, :, None, :]  9.51 us
    dot_general x1, matrix products, state_update(): jnp.einsum('bhvk,bhk->bhv', updated, head_receptance, precision=PRECISE)  8.96 us
    dot_general x1, matrix products, state_update(): removed = jnp.einsum('bhvk,bhk->bhv', matrix, unit_keys, precision=PRECISE)  8.58 us
    mul x3, local copies, waits for them, and re-layouts, state_update(): head_values[..., None] * head_keys[:, :, None, :]  7.99 us
    dot_general x1, matrix products, local(): jnp.einsum('lrf,lfd->lrd', expert_hidden, expert_down_weight, preferred_e...  5.98 us
    reshape x4, local copies, waits for them, and re-layouts, split_heads(): return block.reshape(seq_count, -1, head_width)  5.88 us
  transfers between devices with their start and end apart: 6, of which 4 were waited for; matrix products, arithmetic and copies ran while one was open for 21% of the time, Pallas kernels for 0%

profile of v1, /device:TPU:0, one launch (start us, length us, event | category | flops | bytes accessed | tf_op | source)
XLA Modules:
  0.0 194.7 jit_solution(9931017451690751821)
XLA Ops:
  40.5 3.3 %reshape.173 = f32[32,4,64,64]{3,2,1,0:T(8,128)} reshape(f32[32,4,4096]{2,1,0:T(4,128)S(1)} %copy-done.2) | data formatting | bytes 4194304 | tf_op jit(solution)/shard_map/reshape | solution.py:61
  45.0 8.6 %fusion.70 = f32[32,4,1,64]{3,2,1,0:T(1,128)S(1)} fusion(f32[32,4,64,1]{2,3,1,0:T(1,128)S(1)} %bitcast.88, f32[32,4,64,64]{3,2,1,0:T(8,128)} %reshape.173), kind=kOutput, calls=%fused_computation.92 | convolution fusion | flops 6291456 | bytes 2162688 | tf_op jit(solution)/shard_map/bhvk,bhk->bhv/dot_general | solution.py:62
  53.6 9.0 %fusion.7 = f32[32,4,1,64]{3,2,1,0:T(1,128)} fusion(f32[32,4,64,1]{2,3,1,0:T(1,128)S(1)} %bitcast.94, f32[32,4,64,64]{3,2,1,0:T(8,128)S(1)} %copy-done.1, f32[32,4,64]{2,1,0:T(4,128)S(1)} %copy-done.6, f32[32,4,64]{2,1,0:T(4,128)S(1)} %get-tuple-element.4, f32[32,4,64]{2,1,0:T(4,128)S(1)} %bitcast.86, f32[32,4,64]{2,1,0:T(4,128)S(1)} %copy-done.8, ...), kind=kOutput, calls=%fused_computation.7 | convolution fusion | flops 8912896 | bytes 2326528 | tf_op jit(solution)/shard_map/bhvk,bhk->bhv/dot_general | solution.py:68
  69.0 12.2 %all-gather = bf16[128,2048]{1,0:T(8,128)(2,1)} all-gather(bf16[32,2048]{1,0:T(8,128)(2,1)S(1)} %convolution_convert_fusion.2), channel_id=2, replica_groups=mesh['ep'=8,'tp'=4] {'tp'}, dimensions={0}, use_global_device_ids=true | all-gather | bytes 655360 | tf_op jit(solution)/shard_map/all_gather | solution.py:139
  88.5 4.9 %all-to-all-start = ((bf16[8,16,2048]{2,1,0:T(8,128)(2,1)}), bf16[8,16,2048]{2,1,0:T(8,128)(2,1)}, u32[]{:S(2)}, u32[]{:S(2)}) async-start(bf16[8,16,2048]{2,1,0:T(8,128)(2,1)} %convolution_convert_fusion), calls=%async_computation | async-start | bytes 1048576 | tf_op jit(solution)/shard_map/all_to_all | solution.py:155
  93.4 15.4 %all-to-all-done = bf16[8,16,2048]{2,1,0:T(8,128)(2,1)} async-done(((bf16[8,16,2048]{2,1,0:T(8,128)(2,1)}), bf16[8,16,2048]{2,1,0:T(8,128)(2,1)}, u32[]{:S(2)}, u32[]{:S(2)}) %all-to-all-start) | async-done | bytes 524320 | tf_op jit(solution)/shard_map/all_to_all | solution.py:155
  108.8 3.9 %fusion.5 = f32[128,1024]{1,0:T(8,128)} fusion(bf16[128,2048]{1,0:T(8,128)(2,1)} %bitcast.10, bf16[1,2048,1024]{2,1,0:T(8,128)(2,1)} %param.39), kind=kOutput, calls=%fused_computation.5 | convolution fusion | flops 536870912 | bytes 5242880 | tf_op jit(solution)/shard_map/lrd,ldf->lrf/dot_general | solution.py:160
  112.7 6.0 %fusion.14 = bf16[1,128,2048]{2,1,0:T(8,128)(2,1)} fusion(bf16[1,1024,2048]{2,1,0:T(8,128)(2,1)} %param.41, bf16[128,2048]{1,0:T(8,128)(2,1)} %bitcast.10, bf16[1,2048,1024]{2,1,0:T(8,128)(2,1)} %param.40, f32[128,1024]{1,0:T(8,128)} %fusion.5), kind=kOutput, calls=%fused_computation.13 | convolution fusion | flops 1074790400 | bytes 9961472 | tf_op jit(solution)/shard_map/lrf,lfd->lrd/dot_general | solution.py:167
  120.2 4.2 %all-to-all-start.3 = ((bf16[8,8,2048]{2,1,0:T(8,128)(2,1)}), bf16[8,8,2048]{2,1,0:T(8,128)(2,1)}, u32[]{:S(2)}, u32[]{:S(2)}) async-start(bf16[8,8,2048]{2,1,0:T(8,128)(2,1)} %broadcast_in_dim.2), calls=%async_computation.4 | async-start | bytes 524288 | tf_op jit(solution)/shard_map/all_to_all | solution.py:156
  124.4 3.8 %broadcast_multiply_fusion = f32[32,4,64,64]{3,2,1,0:T(8,128)} fusion(f32[32,4,64]{2,1,0:T(4,128)} %mul.243, f32[32,4,64]{2,1,0:T(4,128)} %mul.240), kind=kLoop, calls=%fused_computation.18 | loop fusion | flops 524288 | bytes 2162688 | tf_op jit(solution)/shard_map/mul | solution.py:66
  128.2 5.1 %mul.277 = f32[32,4,4096]{2,1,0:T(4,128)} reshape(f32[32,4,64,64]{3,2,1,0:T(8,128)} %broadcast_multiply_fusion) | data formatting | bytes 4194304 | tf_op jit(solution)/shard_map/mul | solution.py:66
  133.3 3.8 %broadcast_multiply_fusion.1 = f32[32,4,64,64]{3,2,1,0:T(8,128)} fusion(f32[32,4,64]{2,1,0:T(4,128)} %copy-done.5, f32[32,4,64]{2,1,0:T(4,128)} %bitcast.87), kind=kLoop, calls=%fused_computation.19 | loop fusion | flops 524288 | bytes 2162688 | tf_op jit(solution)/shard_map/mul | solution.py:65
  137.1 5.0 %mul.276 = f32[32,4,4096]{2,1,0:T(4,128)} reshape(f32[32,4,64,64]{3,2,1,0:T(8,128)} %broadcast_multiply_fusion.1) | data formatting | bytes 4194304 | tf_op jit(solution)/shard_map/mul | solution.py:65
  142.1 3.0 %mul.227 = f32[32,4,64,64]{3,2,1,0:T(8,128)} broadcast(f32[32,4,64]{2,1,0:T(4,128)} %mul.226), dimensions={0,1,3} | broadcast | bytes 2129920 | tf_op jit(solution)/shard_map/mul | solution.py:64
  145.2 5.0 %mul.274 = f32[32,4,4096]{2,1,0:T(4,128)} reshape(f32[32,4,64,64]{3,2,1,0:T(8,128)} %mul.227) | data formatting | bytes 4194304 | tf_op jit(solution)/shard_map/mul | solution.py:64
  150.2 2.6 %fusion.44 = f32[64,352]{1,0:T(8,128)} fusion(bf16[2048,352]{0,1:T(8,128)(2,1)} %param.42, bf16[8,8,2048]{2,1,0:T(8,128)(2,1)} %all-to-all-done.3), kind=kOutput, calls=%fused_computation.46 | convolution fusion | flops 92274688 | bytes 1794048 | tf_op jit(solution)/shard_map/dot_general | solution.py:177
  152.8 4.8 %all-to-all-start.1 = ((bf16[8,16,512]{2,1,0:T(8,128)(2,1)}), bf16[8,16,512]{2,1,0:T(8,128)(2,1)}, u32[]{:S(2)}, u32[]{:S(2)}) async-start(bf16[8,16,512]{2,1,0:T(8,128)(2,1)} %bitcast.93), calls=%async_computation.2 | async-start | bytes 262144 | tf_op jit(solution)/shard_map/all_to_all | solution.py:185
  157.7 3.3 %fusion.17 = bf16[8,8,2048]{2,1,0:T(8,128)(2,1)} fusion(bf16[352,2048]{1,0:T(8,128)(2,1)S(1)} %copy-done, bf16[2048,352]{0,1:T(8,128)(2,1)} %param.43, bf16[8,8,2048]{2,1,0:T(8,128)(2,1)} %all-to-all-done.3, f32[64,352]{1,0:T(8,128)} %fusion.44), kind=kOutput, calls=%fused_computation.15 | convolution fusion | flops 184815616 | bytes 3497984 | tf_op jit(solution)/shard_map/dot_general | solution.py:180
  161.0 3.5 %all-to-all-done.1 = bf16[8,16,512]{2,1,0:T(8,128)(2,1)} async-done(((bf16[8,16,512]{2,1,0:T(8,128)(2,1)}), bf16[8,16,512]{2,1,0:T(8,128)(2,1)}, u32[]{:S(2)}, u32[]{:S(2)}) %all-to-all-start.1) | async-done | bytes 131104 | tf_op jit(solution)/shard_map/all_to_all | solution.py:185
  164.5 4.0 %all-to-all-start.4 = ((bf16[8,8,2048]{2,1,0:T(8,128)(2,1)}), bf16[8,8,2048]{2,1,0:T(8,128)(2,1)}, u32[]{:S(2)}, u32[]{:S(2)}) async-start(bf16[8,8,2048]{2,1,0:T(8,128)(2,1)} %fusion.17), calls=%async_computation.5 | async-start | bytes 524288 | tf_op jit(solution)/shard_map/all_to_all | solution.py:186
  168.6 4.7 %subtract_add_fusion = f32[16,8,4096]{2,1,0:T(8,128)} fusion(f32[16,8,4096]{2,1,0:T(8,128)} %bitcast.81, f32[16,8,4096]{2,1,0:T(8,128)} %bitcast.82, f32[16,8,4096]{2,1,0:T(8,128)S(1)} %bitcast.80, f32[16,8,4096]{2,1,0:T(8,128)} %bitcast.83), kind=kLoop, calls=%fused_computation.17 | loop fusion | flops 1572864 | bytes 10485760 | tf_op jit(solution)/shard_map/add | solution.py:64
  175.1 3.2 %all-to-all-done.4 = bf16[8,8,2048]{2,1,0:T(8,128)(2,1)} async-done(((bf16[8,8,2048]{2,1,0:T(8,128)(2,1)}), bf16[8,8,2048]{2,1,0:T(8,128)(2,1)}, u32[]{:S(2)}, u32[]{:S(2)}) %all-to-all-start.4) | async-done | bytes 262176 | tf_op jit(solution)/shard_map/all_to_all | solution.py:186
  178.3 3.3 %all-to-all-start.2 = ((f32[4,8,512]{2,1,0:T(8,128)}), f32[4,8,512]{2,1,0:T(8,128)S(1)}, u32[]{:S(2)}, u32[]{:S(2)}) async-start(f32[4,8,512]{2,1,0:T(8,128)} %convolution_bitcast_fusion), calls=%async_computation.3 | async-start | bytes 131072 | tf_op jit(solution)/shard_map/all_to_all | solution.py:193
  182.5 3.8 %all-to-all-done.2 = f32[4,8,512]{2,1,0:T(8,128)S(1)} async-done(((f32[4,8,512]{2,1,0:T(8,128)}), f32[4,8,512]{2,1,0:T(8,128)S(1)}, u32[]{:S(2)}, u32[]{:S(2)}) %all-to-all-start.2) | async-done | bytes 65568 | tf_op jit(solution)/shard_map/all_to_all | solution.py:193
  (77 shorter events, 53.9 us)
Async XLA Ops:
  7.2 150.5 %copy-start = (bf16[352,2048]{1,0:T(8,128)(2,1)S(1)}, bf16[352,2048]{1,0:T(8,128)(2,1)}, u32[]{:S(2)}) copy-start(bf16[352,2048]{1,0:T(8,128)(2,1)} %param.44) | copy-start | bytes 4325380
  7.2 25.8 %copy-start.10 = (f32[2048]{0:T(1024)S(1)}, f32[2048]{0:T(1024)}, u32[]{:S(2)}) copy-start(f32[2048]{0:T(1024)} %param.25) | copy-start | bytes 24580
  7.2 33.3 %copy-start.2 = (f32[32,4,4096]{2,1,0:T(4,128)S(1)}, f32[32,4,4096]{2,1,0:T(4,128)}, u32[]{:S(2)}) copy-start(f32[32,4,4096]{2,1,0:T(4,128)} %param.24) | copy-start | bytes 6291460
  43.8 9.7 %copy-start.1 = (f32[32,4,64,64]{3,2,1,0:T(8,128)S(1)}, f32[32,4,64,64]{3,2,1,0:T(8,128)}, u32[]{:S(2)}) copy-start(f32[32,4,64,64]{3,2,1,0:T(8,128)} %reshape.173) | copy-start | bytes 6291460
  43.8 9.8 %copy-start.6 = (f32[32,4,64]{2,1,0:T(4,128)S(1)}, f32[32,4,64]{2,1,0:T(4,128)}, u32[]{:S(2)}) copy-start(f32[32,4,64]{2,1,0:T(4,128)} %mul.226) | copy-start | bytes 98308
  43.8 9.8 %copy-start.7 = (f32[32,4,64]{2,1,0:T(4,128)S(1)}, f32[32,4,64]{2,1,0:T(4,128)}, u32[]{:S(2)}) copy-start(f32[32,4,64]{2,1,0:T(4,128)} %mul.240) | copy-start | bytes 98308
  43.8 9.8 %copy-start.8 = (f32[32,4,64]{2,1,0:T(4,128)S(1)}, f32[32,4,64]{2,1,0:T(4,128)}, u32[]{:S(2)}) copy-start(f32[32,4,64]{2,1,0:T(4,128)} %mul.243) | copy-start | bytes 98308
  43.8 9.8 %copy-start.11 = (f32[32,4,64,1]{2,1,0,3:T(4,128)S(1)}, f32[32,4,64,1]{2,1,0,3:T(4,128)}, u32[]{:S(2)}) copy-start(f32[32,4,64,1]{2,1,0,3:T(4,128)} %reshape.186) | copy-start | bytes 98308
  45.0 17.6 %copy-start.5 = (f32[32,4,64]{2,1,0:T(4,128)}, f32[32,4,64]{2,1,0:T(4,128)S(1)}, u32[]{:S(2)}) copy-start(f32[32,4,64]{2,1,0:T(4,128)S(1)} %get-tuple-element.4) | copy-start | bytes 98308
  53.5 9.0 %copy-start.4 = (f32[32,4,1,64]{3,2,1,0:T(1,128)}, f32[32,4,1,64]{3,2,1,0:T(1,128)S(1)}, u32[]{:S(2)}) copy-start(f32[32,4,1,64]{3,2,1,0:T(1,128)S(1)} %fusion.70) | copy-start | bytes 98308
  86.0 1.4 copy-start.3
  88.5 20.3 %all-to-all-start = ((bf16[8,16,2048]{2,1,0:T(8,128)(2,1)}), bf16[8,16,2048]{2,1,0:T(8,128)(2,1)}, u32[]{:S(2)}, u32[]{:S(2)}) async-start(bf16[8,16,2048]{2,1,0:T(8,128)(2,1)} %convolution_convert_fusion), calls=%async_computation | async-start | bytes 1048576 | tf_op jit(solution)/shard_map/all_to_all | solution.py:155
  93.4 59.4 %reduce-scatter.2.cloned.1.call-start = ((), (), s32[]{:S(2)}) async-start(), calls=%async_computation.6 | async-start | bytes 655360 | tf_op jit(solution)/shard_map/reduce_scatter | solution.py:170
  120.2 30.0 %all-to-all-start.3 = ((bf16[8,8,2048]{2,1,0:T(8,128)(2,1)}), bf16[8,8,2048]{2,1,0:T(8,128)(2,1)}, u32[]{:S(2)}, u32[]{:S(2)}) async-start(bf16[8,8,2048]{2,1,0:T(8,128)(2,1)} %broadcast_in_dim.2), calls=%async_computation.4 | async-start | bytes 524288 | tf_op jit(solution)/shard_map/all_to_all | solution.py:156
  152.8 11.7 %all-to-all-start.1 = ((bf16[8,16,512]{2,1,0:T(8,128)(2,1)}), bf16[8,16,512]{2,1,0:T(8,128)(2,1)}, u32[]{:S(2)}, u32[]{:S(2)}) async-start(bf16[8,16,512]{2,1,0:T(8,128)(2,1)} %bitcast.93), calls=%async_computation.2 | async-start | bytes 262144 | tf_op jit(solution)/shard_map/all_to_all | solution.py:185
  164.5 13.8 %all-to-all-start.4 = ((bf16[8,8,2048]{2,1,0:T(8,128)(2,1)}), bf16[8,8,2048]{2,1,0:T(8,128)(2,1)}, u32[]{:S(2)}, u32[]{:S(2)}) async-start(bf16[8,8,2048]{2,1,0:T(8,128)(2,1)} %fusion.17), calls=%async_computation.5 | async-start | bytes 524288 | tf_op jit(solution)/shard_map/all_to_all | solution.py:186
  168.5 4.8 %copy-start.12 = (f32[2048]{0:T(1024)S(1)}, f32[2048]{0:T(1024)}, u32[]{:S(2)}) copy-start(f32[2048]{0:T(1024)} %param.45) | copy-start | bytes 24580
  168.6 4.8 %copy-start.9 = (f32[32,8,16]{0,2,1:T(8,128)S(1)}, f32[32,8,16]{0,2,1:T(8,128)}, u32[]{:S(2)}) copy-start(f32[32,8,16]{0,2,1:T(8,128)} %get-tuple-element.2) | copy-start | bytes 49156
  178.3 8.1 %all-to-all-start.2 = ((f32[4,8,512]{2,1,0:T(8,128)}), f32[4,8,512]{2,1,0:T(8,128)S(1)}, u32[]{:S(2)}, u32[]{:S(2)}) async-start(f32[4,8,512]{2,1,0:T(8,128)} %convolution_bitcast_fusion), calls=%async_computation.3 | async-start | bytes 131072 | tf_op jit(solution)/shard_map/all_to_all | solution.py:193
Sparse Core Ops, SparseCore 0:
  118.8 23.0 reduce-scatter.1
